TPU v7x, 32 devices: a whole 2x2x4 slice. The times are simulated.
32 devices in a mesh: sp: 8 (over z, y), dp: 4 (over x, core).
Axes of the slice: x: 2, y: 2, z: 4, core: 2. Of those that a mesh axis runs over, the one named last changes fastest.
Arguments:
- tokens: bfloat16 [4, 512, 1024], P('dp', 'sp'), may hold values from -6 to 6
- w_query: bfloat16 [1024, 512], P(None, ('sp', 'dp')), may hold values from -0.1875 to 0.1875
- w_forward: bfloat16 [1024, 512], P(None, ('sp', 'dp')), may hold values from -0.1875 to 0.1875
- w_backward: bfloat16 [1024, 512], P(None, ('sp', 'dp')), may hold values from -0.1875 to 0.1875
- w_input: bfloat16 [1024, 512], P(None, ('sp', 'dp')), may hold values from -0.1875 to 0.1875
- w_gate: bfloat16 [1024, 512], P(None, ('sp', 'dp')), may hold values from -0.1875 to 0.1875
- w_out: bfloat16 [512, 1024], P(None, ('sp', 'dp')), may hold values from -0.25 to 0.25
- memory_forward: float32 [512], replicated, may hold values from 0.3 to 4
- memory_backward: float32 [512], replicated, may hold values from 0.3 to 4
- norm_gain: float32 [128], replicated, may hold values from 0.1 to 1.9
Outputs:
- mixed: bfloat16 [4, 512, 1024], P('dp', 'sp')
All inputs are finite; a program needn't handle non-finite values.
Results may differ from a plain program's by a relative error of at most 0.015.
Values may be sent and summed in bfloat16 or wider, within the bound.
A program may use at most 64 MiB of HBM per device.

v0:
```python
import jax
import jax.numpy as jnp
from jax import lax
from jax.sharding import PartitionSpec as P

HEADS = 4
HEAD_DIM = 128
BLOCK = 64
norm_eps = 1e-06
highest = lax.Precision.HIGHEST


def as_sent(array):
    return jax.tree.map(lambda a: a.astype(jnp.bfloat16) if a.dtype == jnp.float32 else a, array)


def gathered_then(share, axis, dim, apply):
    everything = lax.all_gather(share, axis, axis=dim, tiled=True)
    return apply(everything, jnp.int32(0))


def log_forget(projected, memory, seq_len):
    slack_value = memory / seq_len
    return jnp.logaddexp(
        jnp.log1p(-slack_value),
        jnp.log(slack_value) + jax.nn.log_sigmoid(projected.astype(jnp.float32)),
    )


def sweep(queries, log_decay, values):
    seq_len, key_width = queries.shape
    blocks = seq_len // BLOCK
    input_keys = -jnp.expm1(log_decay)
    lower_mask = jnp.tril(jnp.ones((BLOCK, BLOCK), dtype=bool))[:, :, None]

    def advance(carry_state, inputs):
        query_part, decay_part, key_part, value_part = inputs
        running = jnp.cumsum(decay_part, axis=0)
        from_state = jnp.dot(query_part * jnp.exp(running), carry_state, precision=highest)
        gaps = running[:, None, :] - running[None, :, :]
        decay_table = jnp.where(lower_mask, jnp.exp(jnp.where(lower_mask, gaps, 0.0)), 0.0)
        scores = jnp.sum(query_part[:, None, :] * key_part[None, :, :] * decay_table, axis=2)
        inside = jnp.dot(scores, value_part, precision=highest)
        final_sum = running[-1]
        weighted = key_part * jnp.exp(final_sum[None, :] - running)
        carry_state = jnp.exp(final_sum)[:, None] * carry_state + jnp.dot(
            weighted.T, value_part, precision=highest
        )
        return (carry_state, from_state + inside)

    def blocked(array):
        return array.reshape(blocks, BLOCK, array.shape[1])

    zero_state = jnp.zeros((key_width, values.shape[1]), jnp.float32)
    _, readings = lax.scan(
        advance,
        zero_state,
        (blocked(queries), blocked(log_decay), blocked(input_keys), blocked(values)),
    )
    return readings.reshape(seq_len, values.shape[1])


def both_ways(queries, log_ahead, log_behind, values):
    forward_read = sweep(queries, log_ahead, values)
    behind = sweep(jnp.flip(queries, 0), jnp.flip(log_behind, 0), jnp.flip(values, 0))
    return forward_read + jnp.flip(behind, 0)


def body(
    tokens,
    w_query,
    w_forward,
    w_backward,
    w_input,
    w_gate,
    w_out,
    memory_forward,
    memory_backward,
    norm_gain,
):
    seq_count, tok_count, model_width = tokens.shape
    row_count = seq_count * tok_count
    flat_tokens = tokens.reshape(row_count, model_width)
    group_count = lax.axis_size("sp")
    per_head_groups = group_count // HEADS
    block_width = HEAD_DIM // per_head_groups
    head_index = lax.axis_index("sp") // per_head_groups
    full_query, full_forward, full_backward, full_input, full_gate = (
        lax.all_gather(w_query, ("sp", "dp"), axis=1, tiled=True),
        lax.all_gather(w_forward, ("sp", "dp"), axis=1, tiled=True),
        lax.all_gather(w_backward, ("sp", "dp"), axis=1, tiled=True),
        lax.all_gather(w_input, ("sp", "dp"), axis=1, tiled=True),
        lax.all_gather(w_gate, ("sp", "dp"), axis=1, tiled=True),
    )

    def project(weight):
        return jnp.dot(flat_tokens, weight, preferred_element_type=jnp.float32).astype(jnp.bfloat16)

    def by_head(projected):
        shaped = projected.reshape(row_count, HEADS, 1, HEAD_DIM)
        spread_out = jnp.broadcast_to(shaped, (row_count, HEADS, per_head_groups, HEAD_DIM))
        return spread_out.reshape(row_count, group_count, HEAD_DIM)

    def by_group(projected):
        return projected.reshape(row_count, group_count, block_width)

    query_heads, ahead_heads, behind_heads, value_heads = (
        lax.all_to_all(
            as_sent(by_head(project(full_query))), "sp", split_axis=1, concat_axis=0, tiled=True
        ),
        lax.all_to_all(
            as_sent(by_head(project(full_forward))), "sp", split_axis=1, concat_axis=0, tiled=True
        ),
        lax.all_to_all(
            as_sent(by_head(project(full_backward))), "sp", split_axis=1, concat_axis=0, tiled=True
        ),
        lax.all_to_all(
            as_sent(by_group(project(full_input))), "sp", split_axis=1, concat_axis=0, tiled=True
        ),
    )
    gate_rows = project(full_gate)
    seq_len = query_heads.shape[0]
    memory_ahead = lax.dynamic_slice_in_dim(memory_forward, head_index * HEAD_DIM, HEAD_DIM)
    memory_behind = lax.dynamic_slice_in_dim(memory_backward, head_index * HEAD_DIM, HEAD_DIM)
    queries = jax.nn.silu(query_heads[:, 0].astype(jnp.float32))
    log_ahead = log_forget(ahead_heads[:, 0], memory_ahead, seq_len)
    log_behind = log_forget(behind_heads[:, 0], memory_behind, seq_len)
    values = value_heads[:, 0].astype(jnp.float32)
    readout = both_ways(queries, log_ahead, log_behind, values).astype(jnp.bfloat16)
    returned = lax.all_to_all(
        readout.reshape(seq_len, 1, block_width), "sp", split_axis=0, concat_axis=1, tiled=True
    )
    readout_rows = returned.reshape(row_count, HEADS, HEAD_DIM).astype(jnp.float32)
    normed = (
        readout_rows
        * lax.rsqrt(jnp.mean(readout_rows * readout_rows, axis=-1, keepdims=True) + norm_eps)
        * norm_gain
    )
    normed = normed.reshape(row_count, HEADS * HEAD_DIM)
    gated_rows = (normed * jax.nn.silu(gate_rows.astype(jnp.float32))).astype(jnp.bfloat16)

    def output_block(weight_piece, first_index):
        return jnp.dot(gated_rows, weight_piece, preferred_element_type=jnp.float32).astype(
            jnp.bfloat16
        )

    mixed_rows = gathered_then(w_out, ("sp", "dp"), 1, output_block)
    return mixed_rows.reshape(seq_count, tok_count, model_width)


def solution(mesh):
    return jax.shard_map(
        body,
        mesh=mesh,
        in_specs=(
            P("dp", "sp", None),
            P(None, ("sp", "dp")),
            P(None, ("sp", "dp")),
            P(None, ("sp", "dp")),
            P(None, ("sp", "dp")),
            P(None, ("sp", "dp")),
            P(None, ("sp", "dp")),
            P(),
            P(),
            P(),
        ),
        out_specs=P("dp", "sp", None),
        check_vma=False,
    )
```

profile of v0, /device:TPU:0, one launch (start us, length us, event | category | flops | bytes accessed | tf_op | source)
XLA Modules:
  0.0 354.7 jit_solution(13744162278260831660)
XLA Ops:
  12.1 54.5 %all-gather.13.cloned.1.call-done = bf16[1024,512]{0,1:T(8,128)(2,1)} async-done(((bf16[1024,16]{0,1:T(8,128)(2,1)}), bf16[1024,512]{0,1:T(8,128)(2,1)}) %all-gather.13.cloned.1.call-update) | async-done | bytes 1048592 | tf_op jit(solution)/shard_map/all_gather | solution.py:91
  66.6 1.7 fusion.54
  68.2 53.8 %all-gather.9.cloned.1.call-done = bf16[1024,512]{0,1:T(8,128)(2,1)} async-done(((bf16[1024,16]{0,1:T(8,128)(2,1)}), bf16[1024,512]{0,1:T(8,128)(2,1)}) %all-gather.9.cloned.1.call-update) | async-done | bytes 1048592 | tf_op jit(solution)/shard_map/all_gather | solution.py:92
  122.0 1.7 convolution_convert_fusion.4
  124.7 4.5 %all-to-all-start.1 = ((bf16[8,2,2048]{2,1,0:T(2,128)(2,1)}), bf16[8,2,2048]{2,1,0:T(2,128)(2,1)S(1)}, u32[]{:S(2)}, u32[]{:S(2)}) async-start(bf16[8,2,2048]{2,1,0:T(2,128)(2,1)} %reshape.264), calls=%async_computation.1 | async-start | bytes 131072 | tf_op jit(solution)/shard_map/all_to_all | solution.py:117
  129.2 48.4 %all-gather.11.cloned.1.call-done = bf16[1024,512]{0,1:T(8,128)(2,1)} async-done(((bf16[1024,16]{0,1:T(8,128)(2,1)}), bf16[1024,512]{0,1:T(8,128)(2,1)}) %all-gather.11.cloned.1.call-update) | async-done | bytes 1048592 | tf_op jit(solution)/shard_map/all_gather | solution.py:89
  177.5 1.7 fusion.53
  179.2 53.6 %all-gather.7.cloned.1.call-done = bf16[1024,512]{0,1:T(8,128)(2,1)} async-done(((bf16[1024,16]{0,1:T(8,128)(2,1)}), bf16[1024,512]{0,1:T(8,128)(2,1)}) %all-gather.7.cloned.1.call-update) | async-done | bytes 1048592 | tf_op jit(solution)/shard_map/all_gather | solution.py:90
  232.9 1.7 fusion.52
  235.2 4.5 %all-to-all-start.3 = ((bf16[64,8,128]{2,0,1:T(8,128)(2,1)}), bf16[64,8,128]{2,0,1:T(8,128)(2,1)S(1)}, u32[]{:S(2)}, u32[]{:S(2)}) async-start(bf16[64,8,128]{2,0,1:T(8,128)(2,1)} %bitcast.17), calls=%async_computation.3 | async-start | bytes 262144 | tf_op jit(solution)/shard_map/all_to_all | solution.py:114
  240.1 7.1 %all-to-all-done.3 = bf16[64,8,128]{2,0,1:T(8,128)(2,1)S(1)} async-done(((bf16[64,8,128]{2,0,1:T(8,128)(2,1)}), bf16[64,8,128]{2,0,1:T(8,128)(2,1)S(1)}, u32[]{:S(2)}, u32[]{:S(2)}) %all-to-all-start.3) | async-done | bytes 131104 | tf_op jit(solution)/shard_map/all_to_all | solution.py:114
  247.8 3.4 all-to-all-start.2
  251.8 6.7 %all-to-all-done.2 = bf16[64,8,128]{2,0,1:T(8,128)(2,1)S(1)} async-done(((bf16[64,8,128]{2,0,1:T(8,128)(2,1)}), bf16[64,8,128]{2,0,1:T(8,128)(2,1)S(1)}, u32[]{:S(2)}, u32[]{:S(2)}) %all-to-all-start.2) | async-done | bytes 131104 | tf_op jit(solution)/shard_map/all_to_all | solution.py:108
  259.1 3.4 all-to-all-start
  262.8 17.5 %while.29 = (s32[]{:T(128)}, f32[128,64]{0,1:T(8,128)S(1)}, f32[8,64,64]{2,1,0:T(8,128)S(1)}, f32[8,64,128]{2,1,0:T(8,128)S(1)}, f32[8,64,128]{2,1,0:T(8,128)S(1...) while((s32[]{:T(128)}, f32[128,64]{0,1:T(8,128)S(1)}, ...), condition=%wide.region_7.8_spmd.clone.clone, body=%wide.region_4.7_spmd.clone.clone.sunk | while | flops 19451908 | bytes 799868 | solution.py:55
  262.9 1.4 multiply_reduce_fusion.6
  271.6 1.4 multiply_reduce_fusion.6
  280.8 17.5 %while.28 = (s32[]{:T(128)}, f32[128,64]{0,1:T(8,128)S(1)}, f32[8,64,64]{2,1,0:T(8,128)S(1)}, f32[8,64,128]{2,1,0:T(8,128)S(1)}, f32[8,64,128]{2,1,0:T(8,128)S(1...) while((s32[]{:T(128)}, f32[128,64]{0,1:T(8,128)S(1)}, ...), condition=%wide.region_3.4_spmd.clone.clone, body=%wide.region_0.3_spmd.clone.clone.sunk | while | flops 19451908 | bytes 799868 | solution.py:55
  280.9 1.4 multiply_reduce_fusion.5
  294.0 1.4 multiply_reduce_fusion.5
  301.0 5.9 %all-to-all-start.4 = ((bf16[8,2,2048]{2,1,0:T(2,128)(2,1)}), bf16[8,2,2048]{2,1,0:T(2,128)(2,1)S(1)}, u32[]{:S(2)}, u32[]{:S(2)}) async-start(bf16[8,2,2048]{2,1,0:T(2,128)(2,1)} %reshape.266), calls=%async_computation.4 | async-start | bytes 131072 | tf_op jit(solution)/shard_map/all_to_all | solution.py:130
  306.9 6.9 %all-to-all-done.4 = bf16[8,2,2048]{2,1,0:T(2,128)(2,1)S(1)} async-done(((bf16[8,2,2048]{2,1,0:T(2,128)(2,1)}), bf16[8,2,2048]{2,1,0:T(2,128)(2,1)S(1)}, u32[]{:S(2)}, u32[]{:S(2)}) %all-to-all-start.4) | async-done | bytes 65568 | tf_op jit(solution)/shard_map/all_to_all | solution.py:130
  314.7 29.9 %all-gather.17.cloned.1.call-done = bf16[512,1024]{0,1:T(8,128)(2,1)} async-done(((bf16[512,32]{0,1:T(8,128)(2,1)}), bf16[512,1024]{0,1:T(8,128)(2,1)}) %all-gather.17.cloned.1.call-update) | async-done | bytes 1048592 | tf_op jit(solution)/shard_map/all_gather | solution.py:18
  344.8 3.0 fusion.50
  (221 shorter events, 41.8 us)
Async XLA Ops:
  6.5 60.0 %copy-start = (bf16[1,64,1024]{2,1,0:T(8,128)(2,1)S(1)}, bf16[1,64,1024]{2,1,0:T(8,128)(2,1)}, u32[]{:S(2)}) copy-start(bf16[1,64,1024]{2,1,0:T(8,128)(2,1)} %param.14) | copy-start | bytes 393220
  6.5 60.0 %all-gather.13.cloned.1.call-start = ((), (), s32[]{:S(2)}) async-start(), calls=%async_computation.8 | async-start | bytes 1081344 | tf_op jit(solution)/shard_map/all_gather | solution.py:91
  7.3 114.8 %all-gather.9.cloned.1.call-start = ((), (), s32[]{:S(2)}) async-start(), calls=%async_computation.6 | async-start | bytes 1081344 | tf_op jit(solution)/shard_map/all_gather | solution.py:92
  8.0 169.5 %all-gather.11.cloned.1.call-start = ((), (), s32[]{:S(2)}) async-start(), calls=%async_computation.7 | async-start | bytes 1081344 | tf_op jit(solution)/shard_map/all_gather | solution.py:89
  8.7 224.1 %all-gather.7.cloned.1.call-start = ((), (), s32[]{:S(2)}) async-start(), calls=%async_computation.5 | async-start | bytes 1081344 | tf_op jit(solution)/shard_map/all_gather | solution.py:90
  9.3 305.4 %all-gather.15.cloned.1.call-start = ((), (), s32[]{:S(2)}) async-start(), calls=%async_computation.9 | async-start | bytes 1081344 | tf_op jit(solution)/shard_map/all_gather | solution.py:93
  9.9 334.8 %all-gather.17.cloned.1.call-start = ((), (), s32[]{:S(2)}) async-start(), calls=%async_computation.10 | async-start | bytes 1081344 | tf_op jit(solution)/shard_map/all_gather | solution.py:18
  124.7 109.9 %all-to-all-start.1 = ((bf16[8,2,2048]{2,1,0:T(2,128)(2,1)}), bf16[8,2,2048]{2,1,0:T(2,128)(2,1)S(1)}, u32[]{:S(2)}, u32[]{:S(2)}) async-start(bf16[8,2,2048]{2,1,0:T(2,128)(2,1)} %reshape.264), calls=%async_computation.1 | async-start | bytes 131072 | tf_op jit(solution)/shard_map/all_to_all | solution.py:117
  235.2 11.9 %all-to-all-start.3 = ((bf16[64,8,128]{2,0,1:T(8,128)(2,1)}), bf16[64,8,128]{2,0,1:T(8,128)(2,1)S(1)}, u32[]{:S(2)}, u32[]{:S(2)}) async-start(bf16[64,8,128]{2,0,1:T(8,128)(2,1)} %bitcast.17), calls=%async_computation.3 | async-start | bytes 262144 | tf_op jit(solution)/shard_map/all_to_all | solution.py:114
  247.8 10.7 %all-to-all-start.2 = ((bf16[64,8,128]{2,0,1:T(8,128)(2,1)}), bf16[64,8,128]{2,0,1:T(8,128)(2,1)S(1)}, u32[]{:S(2)}, u32[]{:S(2)}) async-start(bf16[64,8,128]{2,0,1:T(8,128)(2,1)} %bitcast.10), calls=%async_computation.2 | async-start | bytes 262144 | tf_op jit(solution)/shard_map/all_to_all | solution.py:108
  259.1 21.2 %all-to-all-start = ((bf16[64,8,128]{2,0,1:T(8,128)(2,1)}), bf16[64,8,128]{2,0,1:T(8,128)(2,1)S(1)}, u32[]{:S(2)}, u32[]{:S(2)}) async-start(bf16[64,8,128]{2,0,1:T(8,128)(2,1)} %bitcast.1), calls=%async_computation | async-start | bytes 262144 | tf_op jit(solution)/shard_map/all_to_all | solution.py:111
  298.2 8.7 %copy-start.1 = (f32[128]{0:T(128)S(1)}, f32[128]{0:T(128)}, u32[]{:S(2)}) copy-start(f32[128]{0:T(128)} %param.23) | copy-start | bytes 1540
  301.0 12.8 %all-to-all-start.4 = ((bf16[8,2,2048]{2,1,0:T(2,128)(2,1)}), bf16[8,2,2048]{2,1,0:T(2,128)(2,1)S(1)}, u32[]{:S(2)}, u32[]{:S(2)}) async-start(bf16[8,2,2048]{2,1,0:T(2,128)(2,1)} %reshape.266), calls=%async_computation.4 | async-start | bytes 131072 | tf_op jit(solution)/shard_map/all_to_all | solution.py:130
Sparse Core Ops, SparseCore 0:
  10.2 56.3 all-gather.12
  69.4 52.5 all-gather.8
  124.9 52.5 all-gather.10
  180.2 52.5 all-gather.6
  235.6 53.3 all-gather.14
  291.7 52.8 all-gather.16
where the time goes:
time: 355 us
  waiting for transfers between devices  265 us (75%)
  other arithmetic  26.9 us (8%)
  starting transfers between devices  21.8 us (6%)
  matrix products  19.3 us (5%)
  between operations  13.8 us (4%)
  local copies, waits for them, and re-layouts  6.91 us (2%)
    all_gather x1, waiting for transfers between devices, body(): lax.all_gather(w_backward, ('sp', 'dp'), axis=1, tiled=True)  54.5 us
    all_gather x1, waiting for transfers between devices, body(): lax.all_gather(w_input, ('sp', 'dp'), axis=1, tiled=True)  53.8 us
    all_gather x1, waiting for transfers between devices, body(): lax.all_gather(w_forward, ('sp', 'dp'), axis=1, tiled=True)  53.6 us
    all_gather x1, waiting for transfers between devices, body(): lax.all_gather(w_query, ('sp', 'dp'), axis=1, tiled=True)  48.4 us
    all_gather x1, waiting for transfers between devices, gathered_then(): everything = lax.all_gather(share, axis, axis=dim, tiled=True)  29.9 us
    reduce_sum x16, other arithmetic, advance(): jnp.sum(query_part[:, None, :] * key_part[None, :, :] * decay_table, axis=2)  21.8 us
  transfers between devices with their start and end apart: 11, of which 8 were waited for; matrix products, arithmetic and copies ran while one was open for 14% of the time, Pallas kernels for 0%

commit v1 on v0

--- a/solution.py
+++ b/solution.py
@@ -86,7 +86,7 @@
     block_width = HEAD_DIM // per_head_groups
     head_index = lax.axis_index("sp") // per_head_groups
     full_query, full_forward, full_backward, full_input, full_gate = (
-        lax.all_gather(w_query, ("sp", "dp"), axis=1, tiled=True),
+        jnp.concatenate(lax.all_gather(w_query, axis_name=("sp", "dp")), axis=1),
         lax.all_gather(w_forward, ("sp", "dp"), axis=1, tiled=True),
         lax.all_gather(w_backward, ("sp", "dp"), axis=1, tiled=True),
         lax.all_gather(w_input, ("sp", "dp"), axis=1, tiled=True),

time: 355 us -> 355 us (level)
    all_gather x1, waiting for transfers between devices: 53.6 us -> 48.2 us  [body(): lax.all_gather(w_forward, ('sp', 'dp'), axis=1, tiled=True)]
    all_gather x1, waiting for transfers between devices: 48.4 us -> 53.8 us  [body(): lax.all_gather(w_query, axis_name=('sp', 'dp'))]
where the time goes in v1:
time: 355 us
  waiting for transfers between devices  263 us (74%)
  other arithmetic  26.9 us (8%)
  starting transfers between devices  21.9 us (6%)
  matrix products  18.1 us (5%)
  between operations  13.8 us (4%)
  local copies, waits for them, and re-layouts  9.3 us (3%)
    all_gather x1, waiting for transfers between devices, body(): lax.all_gather(w_backward, ('sp', 'dp'), axis=1, tiled=True)  54.5 us
    all_gather x1, waiting for transfers between devices, body(): lax.all_gather(w_query, axis_name=('sp', 'dp'))  53.8 us
    all_gather x1, waiting for transfers between devices, body(): lax.all_gather(w_input, ('sp', 'dp'), axis=1, tiled=True)  52.7 us
    all_gather x1, waiting for transfers between devices, body(): lax.all_gather(w_forward, ('sp', 'dp'), axis=1, tiled=True)  48.2 us
    all_gather x1, waiting for transfers between devices, gathered_then(): everything = lax.all_gather(share, axis, axis=dim, tiled=True)  29.9 us
    reduce_sum x16, other arithmetic, advance(): jnp.sum(query_part[:, None, :] * key_part[None, :, :] * decay_table, axis=2)  21.8 us
  transfers between devices with their start and end apart: 11, of which 8 were waited for; matrix products, arithmetic and copies ran while one was open for 14% of the time, Pallas kernels for 0%

profile of v1, /device:TPU:0, one launch (start us, length us, event | category | flops | bytes accessed | tf_op | source)
XLA Modules:
  0.0 354.7 jit_solution(8051969633142091391)
XLA Ops:
  12.1 54.5 %all-gather.12.cloned.1.call-done = bf16[1024,512]{0,1:T(8,128)(2,1)} async-done(((bf16[1024,16]{0,1:T(8,128)(2,1)}), bf16[1024,512]{0,1:T(8,128)(2,1)}) %all-gather.12.cloned.1.call-update) | async-done | bytes 1048592 | tf_op jit(solution)/shard_map/all_gather | solution.py:91
  66.6 1.7 fusion.54
  68.2 53.8 %all-gather.18.cloned.1.call-done = bf16[32768,16]{0,1:T(8,128)(2,1)} async-done(((bf16[1024,16]{0,1:T(8,128)(2,1)}), bf16[32768,16]{0,1:T(8,128)(2,1)}) %all-gather.18.cloned.1.call-update) | async-done | bytes 1048592 | tf_op jit(solution)/shard_map/all_gather | solution.py:89
  122.0 1.8 copy.88
  124.9 52.7 %all-gather.10.cloned.1.call-done = bf16[1024,512]{0,1:T(8,128)(2,1)} async-done(((bf16[1024,16]{0,1:T(8,128)(2,1)}), bf16[1024,512]{0,1:T(8,128)(2,1)}) %all-gather.10.cloned.1.call-update) | async-done | bytes 1048592 | tf_op jit(solution)/shard_map/all_gather | solution.py:92
  177.5 1.7 convolution_convert_fusion.4
  180.2 4.5 %all-to-all-start.1 = ((bf16[8,2,2048]{2,1,0:T(2,128)(2,1)}), bf16[8,2,2048]{2,1,0:T(2,128)(2,1)S(1)}, u32[]{:S(2)}, u32[]{:S(2)}) async-start(bf16[8,2,2048]{2,1,0:T(2,128)(2,1)} %reshape.273), calls=%async_computation.1 | async-start | bytes 131072 | tf_op jit(solution)/shard_map/all_to_all | solution.py:117
  184.7 48.2 %all-gather.8.cloned.1.call-done = bf16[1024,512]{0,1:T(8,128)(2,1)} async-done(((bf16[1024,16]{0,1:T(8,128)(2,1)}), bf16[1024,512]{0,1:T(8,128)(2,1)}) %all-gather.8.cloned.1.call-update) | async-done | bytes 1048592 | tf_op jit(solution)/shard_map/all_gather | solution.py:90
  232.9 1.7 fusion.52
  235.2 4.5 %all-to-all-start.3 = ((bf16[64,8,128]{2,0,1:T(8,128)(2,1)}), bf16[64,8,128]{2,0,1:T(8,128)(2,1)S(1)}, u32[]{:S(2)}, u32[]{:S(2)}) async-start(bf16[64,8,128]{2,0,1:T(8,128)(2,1)} %bitcast.19), calls=%async_computation.3 | async-start | bytes 262144 | tf_op jit(solution)/shard_map/all_to_all | solution.py:114
  240.1 7.1 %all-to-all-done.3 = bf16[64,8,128]{2,0,1:T(8,128)(2,1)S(1)} async-done(((bf16[64,8,128]{2,0,1:T(8,128)(2,1)}), bf16[64,8,128]{2,0,1:T(8,128)(2,1)S(1)}, u32[]{:S(2)}, u32[]{:S(2)}) %all-to-all-start.3) | async-done | bytes 131104 | tf_op jit(solution)/shard_map/all_to_all | solution.py:114
  247.8 3.4 all-to-all-start.2
  251.8 6.7 %all-to-all-done.2 = bf16[64,8,128]{2,0,1:T(8,128)(2,1)S(1)} async-done(((bf16[64,8,128]{2,0,1:T(8,128)(2,1)}), bf16[64,8,128]{2,0,1:T(8,128)(2,1)S(1)}, u32[]{:S(2)}, u32[]{:S(2)}) %all-to-all-start.2) | async-done | bytes 131104 | tf_op jit(solution)/shard_map/all_to_all | solution.py:108
  259.1 3.4 all-to-all-start
  262.8 17.5 %while.29 = (s32[]{:T(128)}, f32[128,64]{0,1:T(8,128)S(1)}, f32[8,64,64]{2,1,0:T(8,128)S(1)}, f32[8,64,128]{2,1,0:T(8,128)S(1)}, f32[8,64,128]{2,1,0:T(8,128)S(1...) while((s32[]{:T(128)}, f32[128,64]{0,1:T(8,128)S(1)}, ...), condition=%wide.region_7.8_spmd.clone.clone, body=%wide.region_4.7_spmd.clone.clone.sunk | while | flops 19451908 | bytes 799868 | solution.py:55
  271.7 1.4 multiply_reduce_fusion.6
  278.2 1.4 multiply_reduce_fusion.6
  280.8 17.5 %while.28 = (s32[]{:T(128)}, f32[128,64]{0,1:T(8,128)S(1)}, f32[8,64,64]{2,1,0:T(8,128)S(1)}, f32[8,64,128]{2,1,0:T(8,128)S(1)}, f32[8,64,128]{2,1,0:T(8,128)S(1...) while((s32[]{:T(128)}, f32[128,64]{0,1:T(8,128)S(1)}, ...), condition=%wide.region_3.4_spmd.clone.clone, body=%wide.region_0.3_spmd.clone.clone.sunk | while | flops 19451908 | bytes 799868 | solution.py:55
  280.9 1.4 multiply_reduce_fusion.5
  294.0 1.4 multiply_reduce_fusion.5
  301.0 5.9 %all-to-all-start.4 = ((bf16[8,2,2048]{2,1,0:T(2,128)(2,1)}), bf16[8,2,2048]{2,1,0:T(2,128)(2,1)S(1)}, u32[]{:S(2)}, u32[]{:S(2)}) async-start(bf16[8,2,2048]{2,1,0:T(2,128)(2,1)} %reshape.275), calls=%async_computation.4 | async-start | bytes 131072 | tf_op jit(solution)/shard_map/all_to_all | solution.py:130
  306.9 6.9 %all-to-all-done.4 = bf16[8,2,2048]{2,1,0:T(2,128)(2,1)S(1)} async-done(((bf16[8,2,2048]{2,1,0:T(2,128)(2,1)}), bf16[8,2,2048]{2,1,0:T(2,128)(2,1)S(1)}, u32[]{:S(2)}, u32[]{:S(2)}) %all-to-all-start.4) | async-done | bytes 65568 | tf_op jit(solution)/shard_map/all_to_all | solution.py:130
  314.8 29.9 %all-gather.16.cloned.1.call-done = bf16[512,1024]{0,1:T(8,128)(2,1)} async-done(((bf16[512,32]{0,1:T(8,128)(2,1)}), bf16[512,1024]{0,1:T(8,128)(2,1)}) %all-gather.16.cloned.1.call-update) | async-done | bytes 1048592 | tf_op jit(solution)/shard_map/all_gather | solution.py:18
  344.8 3.0 fusion.50
  (223 shorter events, 42.8 us)
Async XLA Ops:
  6.5 60.0 %copy-start = (bf16[1,64,1024]{2,1,0:T(8,128)(2,1)S(1)}, bf16[1,64,1024]{2,1,0:T(8,128)(2,1)}, u32[]{:S(2)}) copy-start(bf16[1,64,1024]{2,1,0:T(8,128)(2,1)} %param.14) | copy-start | bytes 393220
  6.5 60.0 %all-gather.12.cloned.1.call-start = ((), (), s32[]{:S(2)}) async-start(), calls=%async_computation.7 | async-start | bytes 1081344 | tf_op jit(solution)/shard_map/all_gather | solution.py:91
  7.3 114.8 %all-gather.18.cloned.1.call-start = ((), (), s32[]{:S(2)}) async-start(), calls=%async_computation.10 | async-start | bytes 1081344 | tf_op jit(solution)/shard_map/all_gather | solution.py:89
  8.0 169.5 %all-gather.10.cloned.1.call-start = ((), (), s32[]{:S(2)}) async-start(), calls=%async_computation.6 | async-start | bytes 1081344 | tf_op jit(solution)/shard_map/all_gather | solution.py:92
  8.7 224.1 %all-gather.8.cloned.1.call-start = ((), (), s32[]{:S(2)}) async-start(), calls=%async_computation.5 | async-start | bytes 1081344 | tf_op jit(solution)/shard_map/all_gather | solution.py:90
  9.3 305.4 %all-gather.14.cloned.1.call-start = ((), (), s32[]{:S(2)}) async-start(), calls=%async_computation.8 | async-start | bytes 1081344 | tf_op jit(solution)/shard_map/all_gather | solution.py:93
  9.9 334.8 %all-gather.16.cloned.1.call-start = ((), (), s32[]{:S(2)}) async-start(), calls=%async_computation.9 | async-start | bytes 1081344 | tf_op jit(solution)/shard_map/all_gather | solution.py:18
  180.2 54.4 %all-to-all-start.1 = ((bf16[8,2,2048]{2,1,0:T(2,128)(2,1)}), bf16[8,2,2048]{2,1,0:T(2,128)(2,1)S(1)}, u32[]{:S(2)}, u32[]{:S(2)}) async-start(bf16[8,2,2048]{2,1,0:T(2,128)(2,1)} %reshape.273), calls=%async_computation.1 | async-start | bytes 131072 | tf_op jit(solution)/shard_map/all_to_all | solution.py:117
  235.2 11.9 %all-to-all-start.3 = ((bf16[64,8,128]{2,0,1:T(8,128)(2,1)}), bf16[64,8,128]{2,0,1:T(8,128)(2,1)S(1)}, u32[]{:S(2)}, u32[]{:S(2)}) async-start(bf16[64,8,128]{2,0,1:T(8,128)(2,1)} %bitcast.19), calls=%async_computation.3 | async-start | bytes 262144 | tf_op jit(solution)/shard_map/all_to_all | solution.py:114
  247.8 10.7 %all-to-all-start.2 = ((bf16[64,8,128]{2,0,1:T(8,128)(2,1)}), bf16[64,8,128]{2,0,1:T(8,128)(2,1)S(1)}, u32[]{:S(2)}, u32[]{:S(2)}) async-start(bf16[64,8,128]{2,0,1:T(8,128)(2,1)} %bitcast.12), calls=%async_computation.2 | async-start | bytes 262144 | tf_op jit(solution)/shard_map/all_to_all | solution.py:108
  259.1 21.2 %all-to-all-start = ((bf16[64,8,128]{2,0,1:T(8,128)(2,1)}), bf16[64,8,128]{2,0,1:T(8,128)(2,1)S(1)}, u32[]{:S(2)}, u32[]{:S(2)}) async-start(bf16[64,8,128]{2,0,1:T(8,128)(2,1)} %bitcast.1), calls=%async_computation | async-start | bytes 262144 | tf_op jit(solution)/shard_map/all_to_all | solution.py:111
  298.3 8.7 %copy-start.1 = (f32[128]{0:T(128)S(1)}, f32[128]{0:T(128)}, u32[]{:S(2)}) copy-start(f32[128]{0:T(128)} %param.23) | copy-start | bytes 1540
  301.0 12.8 %all-to-all-start.4 = ((bf16[8,2,2048]{2,1,0:T(2,128)(2,1)}), bf16[8,2,2048]{2,1,0:T(2,128)(2,1)S(1)}, u32[]{:S(2)}, u32[]{:S(2)}) async-start(bf16[8,2,2048]{2,1,0:T(2,128)(2,1)} %reshape.275), calls=%async_computation.4 | async-start | bytes 131072 | tf_op jit(solution)/shard_map/all_to_all | solution.py:130
Sparse Core Ops, SparseCore 0:
  10.2 56.3 all-gather.11
  69.5 52.5 all-gather.17
  124.9 52.5 all-gather.9
  180.3 52.5 all-gather.7
  235.6 53.3 all-gather.13
  291.7 52.8 all-gather.15
